TPU v7x, 32 devices: a whole 2x2x4 slice. The times are simulated.
32 devices in a mesh: fs: 8 (over z, y), tp: 4 (over x, core).
Axes of the slice: x: 2, y: 2, z: 4, core: 2. Of those that a mesh axis runs over, the one named last changes fastest.
Arguments:
- tokens: bfloat16 [3072, 2048], P('tp'), may hold values from -6 to 6
- norm_gain: float32 [2048], P('fs'), may hold values from 0.1 to 1.9
- gate_weight: float32 [4, 2048, 8192], P(None, 'fs', 'tp'), may hold values from -0.125 to 0.125
- up_weight: float32 [4, 2048, 8192], P(None, 'fs', 'tp'), may hold values from -0.125 to 0.125
- down_weight: float32 [4, 8192, 2048], P(None, 'fs', 'tp'), may hold values from -0.0625 to 0.0625
- routes: int32 [3072, 2], P('tp'), may hold values from 0 to 3, all different within a row; in each aligned block of 768 rows (0 to 767, 768 to 1535, ...) at most 480 rows name the same one
- route_logit: float32 [3072, 2], P('tp'), may hold values from -6 to 6
Outputs:
- gate_out: bfloat16 [4, 2048, 8192], P(None, None, 'fs')
- up_out: bfloat16 [4, 2048, 8192], P(None, None, 'fs')
- down_out: bfloat16 [4, 8192, 2048], P(None, 'fs')
- mixed: bfloat16 [3072, 2048], P(('tp', 'fs'))
Inputs may be any that keep to these rules, and one draw needn't show every extreme that they name: `routes`: the two experts of a token differ. In each aligned block of 768 tokens (the tokens of one request group) every expert is named by at most 480 tokens, a bound that some block reaches.
All inputs are finite; a program needn't handle non-finite values.
Results may differ from a plain program's by a relative error of at most 0.0082.
Values may be sent and summed in bfloat16 or wider, within the bound.
A program may use at most 192 MiB of HBM per device.

v0:
```python
import jax
import jax.numpy as jnp
from jax import lax
from jax.sharding import PartitionSpec as P

EPS = 0.5


def shards(tokens, norm_gain, gate_weight, up_weight, down_weight, routes, route_logit):
    gain_col = norm_gain[None, :, None]
    gate_part = (gate_weight * gain_col).astype(jnp.bfloat16)
    up_part = (up_weight * gain_col).astype(jnp.bfloat16)
    down_part = down_weight.astype(jnp.bfloat16)
    gate_one, up_one = (
        lax.all_to_all(gate_part, "tp", split_axis=0, concat_axis=2, tiled=True),
        lax.all_to_all(up_part, "tp", split_axis=0, concat_axis=2, tiled=True),
    )
    gate_mine, up_mine = (
        lax.all_to_all(gate_one, "fs", split_axis=2, concat_axis=1, tiled=True),
        lax.all_to_all(up_one, "fs", split_axis=2, concat_axis=1, tiled=True),
    )
    gate_out, up_out = (
        lax.all_gather(gate_mine, "tp", axis=0, tiled=True),
        lax.all_gather(up_mine, "tp", axis=0, tiled=True),
    )
    down_out = lax.all_gather(down_part, "tp", axis=2, tiled=True)
    total_rows = tokens.shape[0]
    width = tokens.shape[1]
    experts = gate_out.shape[0]
    capacity = total_rows * 5 // 8
    floats = tokens.astype(jnp.float32)
    normed = (floats * lax.rsqrt(jnp.mean(floats * floats, axis=1, keepdims=True) + EPS)).astype(
        jnp.bfloat16
    )
    first_share = jax.nn.sigmoid(route_logit[:, 0] - route_logit[:, 1])
    shares = jnp.stack([first_share, 1.0 - first_share], axis=1)
    chosen = (routes[:, :, None] == jnp.arange(experts, dtype=jnp.int32)[None, None, :]).astype(
        jnp.int32
    )
    counts = jnp.sum(chosen, axis=1)
    before = jnp.cumsum(counts, axis=0) - counts
    slot_index = jnp.sum(chosen * before[:, None, :], axis=2)
    flat_slot = routes * capacity + slot_index
    row_ids = jnp.repeat(jnp.arange(total_rows, dtype=jnp.int32), 2)
    table = (
        jnp.full((experts * capacity,), total_rows, jnp.int32)
        .at[flat_slot.reshape(-1)]
        .set(row_ids)
    )
    gathered = jnp.take(normed, table, axis=0, mode="fill", fill_value=0).reshape(
        experts, capacity, width
    )
    gate_val = jnp.einsum("ecd,edf->ecf", gathered, gate_out, preferred_element_type=jnp.float32)
    up_val = jnp.einsum("ecd,edf->ecf", gathered, up_out, preferred_element_type=jnp.float32)
    hidden = (jax.nn.silu(gate_val) * up_val).astype(jnp.bfloat16)
    results = jnp.einsum("ecf,efd->ecd", hidden, down_out, preferred_element_type=jnp.float32)
    flat_rows = results.reshape(experts * capacity, width)
    first_rows = jnp.take(flat_rows, flat_slot[:, 0], axis=0)
    second_rows = jnp.take(flat_rows, flat_slot[:, 1], axis=0)
    mixed = lax.psum_scatter(
        shares[:, 0:1] * first_rows + shares[:, 1:2] * second_rows,
        "fs",
        scatter_dimension=0,
        tiled=True,
    )
    return (gate_out, up_out, down_out, mixed.astype(jnp.bfloat16))


def solution(mesh):
    return jax.shard_map(
        shards,
        mesh=mesh,
        in_specs=(
            P("tp", None),
            P("fs"),
            P(None, "fs", "tp"),
            P(None, "fs", "tp"),
            P(None, "fs", "tp"),
            P("tp", None),
            P("tp", None),
        ),
        out_specs=(
            P(None, None, "fs"),
            P(None, None, "fs"),
            P(None, "fs", None),
            P(("tp", "fs"), None),
        ),
        check_vma=False,
    )
```

profile of v0, /device:TPU:0, one launch (start us, length us, event | category | flops | bytes accessed | tf_op | source)
XLA Modules:
  0.0 959.0 jit_solution(9687158230475078291)
XLA Ops:
  7.2 8.7 copy.43
  15.9 8.7 copy.46
  24.6 10.7 %multiply_convert_fusion = (bf16[4,256,2048]{1,2,0:T(8,128)(2,1)}, bf16[4,256,2048]{1,2,0:T(8,128)(2,1)}) fusion(f32[4,256,2048]{1,2,0:T(8,128)} %copy.46, f32[256]{0:T(256)S(1)} %copy-done.3, f32[4,256,2048]{1,2,0:T(8,128)} %copy.43), kind=kLoop, calls=%fused_computation.4 | loop fusion | flops 8388608 | bytes 25166848 | tf_op jit(solution)/shard_map/convert_element_type | solution.py:12
  35.3 52.6 %all_to_all.72 = bf16[4,256,2048]{1,2,0:T(8,128)(2,1)S(1)} all-to-all(bf16[4,256,2048]{1,2,0:T(8,128)(2,1)} %get-tuple-element.9), channel_id=1, replica_groups=mesh['fs'=8,'tp'=4] {'tp'}, dimensions={0} | all-to-all | bytes 8388608 | tf_op jit(solution)/shard_map/all_to_all | solution.py:16
  87.9 49.3 %copy.56 = bf16[1,256,8192]{1,0,2:T(2,128)(2,1)} copy(bf16[1,256,8192]{1,2,0:T(8,128)(2,1)S(1)} %bitcast.49) | data formatting | bytes 8388608 | tf_op jit(solution)/shard_map/all_to_all | solution.py:16
  137.7 43.5 %reduce.13 = bf16[8192,256]{1,0:T(8,128)(2,1)} reduce(bf16[8192,1,256]{2,1,0:T(2,128)(2,1)} %bitcast.45, bf16[]{:T(256)} %broadcast.78), dimensions={1}, to_apply=%bitcast.40.reduce_sub_computation | reduce | bytes 8388610
  188.2 99.8 %all_to_all.73 = bf16[8,2,131072]{2,1,0:T(2,128)(2,1)} all-to-all(bf16[8,2,131072]{2,1,0:T(2,128)(2,1)} %reshape.137), channel_id=1, replica_groups=mesh['fs'=8,'tp'=4] {'fs'}, dimensions={0} | all-to-all | bytes 8388608 | tf_op jit(solution)/shard_map/all_to_all | solution.py:20
  288.0 8.7 reshape.138
  315.4 97.4 %all_to_all.74 = bf16[4,256,2048]{1,2,0:T(8,128)(2,1)S(1)} all-to-all(bf16[4,256,2048]{1,2,0:T(8,128)(2,1)} %get-tuple-element.10), channel_id=1, replica_groups=mesh['fs'=8,'tp'=4] {'tp'}, dimensions={0} | all-to-all | bytes 8388608 | tf_op jit(solution)/shard_map/all_to_all | solution.py:15
  412.8 49.3 %copy.57 = bf16[1,256,8192]{1,0,2:T(2,128)(2,1)} copy(bf16[1,256,8192]{1,2,0:T(8,128)(2,1)S(1)} %bitcast.51) | data formatting | bytes 8388608 | tf_op jit(solution)/shard_map/all_to_all | solution.py:15
  462.2 43.5 %reduce.12 = bf16[8192,256]{1,0:T(8,128)(2,1)} reduce(bf16[8192,1,256]{2,1,0:T(2,128)(2,1)} %bitcast.46, bf16[]{:T(256)} %broadcast.78), dimensions={1}, to_apply=%bitcast.41.reduce_sub_computation | reduce | bytes 8388610
  505.7 7.0 reshape.135
  512.7 97.7 %all_to_all.75 = bf16[8,2,131072]{2,1,0:T(2,128)(2,1)} all-to-all(bf16[8,2,131072]{2,1,0:T(2,128)(2,1)} %reshape.135), channel_id=1, replica_groups=mesh['fs'=8,'tp'=4] {'fs'}, dimensions={0} | all-to-all | bytes 8388608 | tf_op jit(solution)/shard_map/all_to_all | solution.py:19
  610.4 8.7 reshape.136
  644.9 8.9 gather_fusion
  654.0 16.3 %fusion = f32[4,480,1024]{2,1,0:T(8,128)} fusion(bf16[4,2048,1024]{2,1,0:T(8,128)(2,1)} %all-gather.6.cloned.1.call-done, bf16[4,480,2048]{2,1,0:T(8,128)(2,1)} %bitcast.57, pred[4,480]{1,0:T(4,128)(4,1)S(1)} %broadcast_in_dim.37), kind=kOutput, calls=%fused_computation.10 | convolution fusion | flops 8056995840 | bytes 32507776 | tf_op jit(solution)/shard_map/ecd,edf->ecf/dot_general | solution.py:54
  670.2 65.7 %all-gather.4.cloned.1.call-done = bf16[4,2048,1024]{2,1,0:T(8,128)(2,1)} async-done(((bf16[1,2048,1024]{2,1,0:T(8,128)(2,1)}), bf16[4,2048,1024]{2,1,0:T(8,128)(2,1)}) %all-gather.4.cloned.1.call-update) | async-done | bytes 16777232 | tf_op jit(solution)/shard_map/all_gather | solution.py:23
  735.9 27.2 %fusion.7 = f32[4,480,2048]{2,1,0:T(8,128)} fusion(bf16[4,1024,2048]{2,1,0:T(8,128)(2,1)} %all-gather.8.cloned.1.call-done, f32[4,480,1024]{2,1,0:T(8,128)} %fusion, bf16[4,2048,1024]{2,1,0:T(8,128)(2,1)} %all-gather.4.cloned.1.call-done, bf16[4,480,2048]{2,1,0:T(8,128)(2,1)} %bitcast.58, pred[4,480]{1,0:T(4,128)(4,1)S(1)} %broadcast_in_dim.37), kind=kOutput, calls=%fused_computation.19 | convolution fusion | flops 16121856000 | bytes 65013632 | tf_op jit(solution)/shard_map/ecf,efd->ecd/dot_general | solution.py:56
  763.1 12.7 %gather_fusion.1 = f32[768,2048]{1,0:T(8,128)} fusion(f32[1920,2048]{1,0:T(8,128)} %bitcast.43, s32[1024]{0:T(1024)S(1)} %pad_clamp_fusion.2), kind=kCustom, calls=%fused_computation.clone | custom fusion | bytes 12585984 | tf_op jit(solution)/shard_map/jit(_take)/gather | solution.py:58
  775.8 12.7 %gather_fusion.2 = f32[768,2048]{1,0:T(8,128)} fusion(f32[1920,2048]{1,0:T(8,128)} %bitcast.44, s32[1024]{0:T(1024)S(1)} %pad_clamp_fusion.1), kind=kCustom, calls=%fused_computation.1.clone | custom fusion | bytes 12585984 | tf_op jit(solution)/shard_map/jit(_take)/gather | solution.py:59
  788.5 7.2 fusion.4
  795.7 118.2 %reduce-scatter.2.cloned.1.call-done = f32[96,2048]{1,0:T(8,128)} async-done(((f32[768,2048]{1,0:T(8,128)}), f32[96,2048]{1,0:T(8,128)}) %reduce-scatter.2.cloned.1.call-update) | async-done | bytes 786448 | tf_op jit(solution)/shard_map/reduce_scatter | solution.py:60
  915.8 15.2 %copy.61 = bf16[4,2048,1024]{2,1,0:T(8,128)(2,1)} copy(bf16[4,2048,1024]{2,1,0:T(8,128)(2,1)} %all-gather.4.cloned.1.call-done) | data formatting | bytes 33554432
  931.1 15.2 %copy.62 = bf16[4,2048,1024]{2,1,0:T(8,128)(2,1)} copy(bf16[4,2048,1024]{2,1,0:T(8,128)(2,1)} %all-gather.6.cloned.1.call-done) | data formatting | bytes 33554432
  (64 shorter events, 60.2 us)
Async XLA Ops:
  7.2 646.8 %all-gather.6.cloned.1.call-start = ((), (), s32[]{:S(2)}) async-start(), calls=%async_computation.6 | async-start | bytes 20971520 | tf_op jit(solution)/shard_map/all_gather | solution.py:24
  15.9 8.7 copy-start.3
  309.3 360.9 %all-gather.8.cloned.1.call-start = ((), (), s32[]{:S(2)}) async-start(), calls=%async_computation.7 | async-start | bytes 20971520 | tf_op jit(solution)/shard_map/all_gather | solution.py:26
  315.4 420.5 %all-gather.4.cloned.1.call-start = ((), (), s32[]{:S(2)}) async-start(), calls=%async_computation.5 | async-start | bytes 20971520 | tf_op jit(solution)/shard_map/all_gather | solution.py:23
  625.2 6.7 copy-start.1
  625.2 16.2 %copy-start = (bf16[768,2048]{1,0:T(8,128)(2,1)S(1)}, bf16[768,2048]{1,0:T(8,128)(2,1)}, u32[]{:S(2)}) copy-start(bf16[768,2048]{1,0:T(8,128)(2,1)} %param.9) | copy-start | bytes 9437188
  631.8 282.1 %reduce-scatter.2.cloned.1.call-start = ((), (), s32[]{:S(2)}) async-start(), calls=%async_computation.8 | async-start | bytes 7077888 | tf_op jit(solution)/shard_map/reduce_scatter | solution.py:60
  644.9 8.9 copy-start.2
  915.8 30.5 %slice-start = ((s8[16777216]{0:T(1024)(128)(4,1)}), s8[4194304]{0:T(1024)(128)(4,1)S(1)}, s32[]{:S(2)}) async-start(s8[16777216]{0:T(1024)(128)(4,1)} %bitcast.53), calls=%async_computation.9 | async-start | bytes 8388608
  915.8 30.5 %slice-start.1 = ((s8[16777216]{0:T(1024)(128)(4,1)}), s8[4194304]{0:T(1024)(128)(4,1)S(1)}, s32[]{:S(2)}) async-start(s8[16777216]{0:T(1024)(128)(4,1)} %bitcast.53), calls=%async_computation.10 | async-start | bytes 8388608
  931.1 15.2 %slice-start.2 = ((s8[16777216]{0:T(1024)(128)(4,1)}), s8[4194304]{0:T(1024)(128)(4,1)S(1)}, s32[]{:S(2)}) async-start(s8[16777216]{0:T(1024)(128)(4,1)} %bitcast.53), calls=%async_computation.11 | async-start | bytes 8388608
  931.1 15.2 %slice-start.3 = ((s8[16777216]{0:T(1024)(128)(4,1)}), s8[4194304]{0:T(1024)(128)(4,1)S(1)}, s32[]{:S(2)}) async-start(s8[16777216]{0:T(1024)(128)(4,1)} %bitcast.53), calls=%async_computation.12 | async-start | bytes 8388608
Sparse Core Ops, SparseCore 0:
  309.4 148.9 all-gather.5
  460.0 104.8 all-gather.7
  631.9 103.9 all-gather.3
  795.8 118.0 reduce-scatter.1
where the time goes:
time: 961 us; the launch traced here: 959 us
  blocking collectives  347 us (36%)
  local copies, waits for them, and re-layouts  252 us (26%)
  waiting for transfers between devices  184 us (19%)
  other arithmetic  118 us (12%)
  matrix products  43.5 us (5%)
  between operations  14 us (1%)
    reduce_scatter x1, waiting for transfers between devices, shards(): lax.psum_scatter(shares[:, 0:1] * first_rows + shares[:, 1:2] * second_ro...  118 us
    all_to_all x1, blocking collectives, shards(): lax.all_to_all(up_one, 'fs', split_axis=2, concat_axis=1, tiled=True)  99.8 us
    unnamed x28, local copies, waits for them, and re-layouts  98.2 us
    all_to_all x1, blocking collectives, shards(): lax.all_to_all(gate_one, 'fs', split_axis=2, concat_axis=1, tiled=True)  97.7 us
    all_to_all x1, blocking collectives, shards(): lax.all_to_all(gate_part, 'tp', split_axis=0, concat_axis=2, tiled=True)  97.4 us
    unnamed x4, other arithmetic  87.2 us
    all_gather x1, waiting for transfers between devices, shards(): lax.all_gather(gate_mine, 'tp', axis=0, tiled=True)  65.7 us
    all_to_all x1, blocking collectives, shards(): lax.all_to_all(up_part, 'tp', split_axis=0, concat_axis=2, tiled=True)  52.6 us
  transfers between devices with their start and end apart: 4, of which 2 were waited for; matrix products, arithmetic and copies ran while one was open for 17% of the time, Pallas kernels for 0%

commit v1 on v0

v1 whole, which is shorter than its diff:
```python
import functools

import jax
import jax.numpy as jnp
from jax import lax
from jax.experimental import pallas as pl
from jax.experimental.pallas import tpu as pltpu
from jax.sharding import PartitionSpec as P

EPS = 0.5
MESH = pl.DeviceIdType.MESH
VMEM_LIMIT = 62 * 1024 * 1024


def spread(
    fs_size, tp_size,
    gate, up, down,
    gate_all, up_all, down_all, gate_far, up_far,
    across_send, across_recv, near_send, near_recv, far_send, twin_send, twin_recv,
    down_send, down_recv,
):
    experts, depth, width = gate.shape
    units = gate_all.shape[2]
    per = width // units
    fs, tp = lax.axis_index("fs"), lax.axis_index("tp")
    half, side = tp // 2, tp % 2
    twin = half * 2 + 1 - side
    across = (1 - half) * 2 + side
    col = down.shape[2]

    def remote(src, dst, send, recv, fs_to, tp_to):
        return pltpu.make_async_remote_copy(
            src_ref=src, dst_ref=dst, send_sem=send, recv_sem=recv,
            device_id=(fs_to, tp_to), device_id_type=MESH,
        )

    def columns(owner):
        return pl.ds(pl.multiple_of(owner * col, col), col)

    pieces = [(a, e) for e in range(experts) for a in range(2)]
    own, far, full = (gate, up), (gate_far, up_far), (gate_all, up_all)

    crossing = []
    for a, e in pieces:
        copy = remote(
            own[a].at[e], far[a].at[e], across_send.at[a, e], across_recv.at[a, e], fs, across
        )
        copy.start()
        crossing.append(copy)

    rows = pl.ds(pl.multiple_of(fs * depth, depth), depth)

    def deal(source, a, e, owner, sem):
        for h in range(per):
            remote(
                source[a].at[e, :, pl.ds(h * units, units)],
                full[a].at[e, rows, :],
                sem.at[a, e],
                near_recv.at[a, e],
                owner * per + h,
                twin,
            ).start()

    for a, e in pieces:
        deal(own, a, e, tp, near_send)

    down_near = remote(
        down, down_all.at[:, :, columns(tp)], down_send.at[0], down_recv.at[0], fs, twin
    )
    down_near.start()
    down_far = remote(
        down, down_all.at[:, :, columns(tp)], down_send.at[1], down_recv.at[1], fs, across
    )
    down_far.start()

    for (a, e), copy in zip(pieces, crossing):
        copy.wait_recv()
        deal(far, a, e, across, far_send)

    def hand_down(owner, index):
        return remote(
            down_all.at[:, :, columns(owner)], down_all.at[:, :, columns(owner)],
            down_send.at[index], down_recv.at[index], fs, twin,
        )

    down_near.wait_recv()
    echo = hand_down(twin, 2)
    echo.start()
    down_far.wait_recv()
    passed = hand_down(across, 3)
    passed.start()

    lands = side == 1 - (fs // per) % 2

    def hand(a, e):
        return remote(
            full[a].at[e], full[a].at[e], twin_send.at[a, e], twin_recv.at[a, e], fs, twin
        )

    @pl.when(lands)
    def _():
        for a, e in pieces:
            pltpu.make_async_copy(full[a].at[e], full[a].at[e], near_recv.at[a, e]).wait()
            hand(a, e).start()
        for a, e in pieces:
            hand(a, e).wait_send()

    @pl.when(jnp.logical_not(lands))
    def _():
        for a, e in pieces:
            hand(a, e).wait_recv()

    for (a, e), copy in zip(pieces, crossing):
        copy.wait_send()
        pltpu.make_async_copy(own[a].at[e], own[a].at[e], near_send.at[a, e]).wait()
        pltpu.make_async_copy(far[a].at[e], far[a].at[e], far_send.at[a, e]).wait()
    down_near.wait_send()
    down_far.wait_send()
    echo.wait()
    passed.wait()


def apply_experts(x, weight, gate, up, down, gate_out, up_out, down_out, part, total):
    expert, block = pl.program_id(0), pl.program_id(1)
    gate_out[...] = gate[...]
    up_out[...] = up[...]
    down_out[...] = down[...]
    rows = x.shape[0]
    tile = rows // 2

    @pl.when(jnp.logical_and(expert == 0, block == 0))
    def _():
        total[...] = jnp.zeros_like(total)

    def step(i, carry):
        at = pl.ds(pl.multiple_of(i * tile, tile), tile)
        mine = x[at, :]
        gate_val = jnp.dot(mine, gate[0], preferred_element_type=jnp.float32)
        up_val = jnp.dot(mine, up[0], preferred_element_type=jnp.float32)
        hidden = (jax.nn.silu(gate_val) * up_val).astype(jnp.bfloat16)
        result = jnp.dot(hidden, down[0], preferred_element_type=jnp.float32)
        shares = weight[at, :]
        lane = lax.broadcasted_iota(jnp.int32, shares.shape, 1)
        share = jnp.sum(jnp.where(lane == expert, shares, 0.0), axis=1, keepdims=True)
        total[at, :] += share * result
        return carry

    lax.fori_loop(0, rows // tile, step, 0)

    @pl.when(
        jnp.logical_and(expert == pl.num_programs(0) - 1, block == pl.num_programs(1) - 1)
    )
    def _():
        part[...] = total[...].astype(part.dtype)


def fold(chunks, part, out, low_in, mid, high_in, low_send, low_recv, high_send, high_recv):
    highs, _, rows, width = part.shape
    step = width // chunks
    fs, tp = lax.axis_index("fs"), lax.axis_index("tp")
    high, low = fs // 2, fs % 2
    first = []
    for k in range(chunks):
        copy = pltpu.make_async_remote_copy(
            src_ref=part.at[:, 1 - low, :, pl.ds(k * step, step)],
            dst_ref=low_in.at[k],
            send_sem=low_send.at[k],
            recv_sem=low_recv.at[k],
            device_id=(high * 2 + 1 - low, tp),
            device_id_type=MESH,
        )
        copy.start()
        first.append(copy)
    second = []
    for k in range(chunks):
        first[k].wait_recv()
        mid[k] = (
            part[:, low, :, pl.ds(k * step, step)].astype(jnp.float32)
            + low_in[k].astype(jnp.float32)
        ).astype(mid.dtype)
        for shift in range(1, highs):
            to = lax.rem(high + shift, highs)
            copy = pltpu.make_async_remote_copy(
                src_ref=mid.at[k, to],
                dst_ref=high_in.at[k, shift],
                send_sem=high_send.at[k, shift],
                recv_sem=high_recv.at[k, shift],
                device_id=(to * 2 + low, tp),
                device_id_type=MESH,
            )
            copy.start()
            second.append((k, copy))
    for k in range(chunks):
        total = part[high, low, :, pl.ds(k * step, step)].astype(jnp.float32) + low_in[
            k, high
        ].astype(jnp.float32)
        shift = 0
        for at, copy in second:
            if at == k:
                shift += 1
                copy.wait_recv()
                total = total + high_in[k, shift].astype(jnp.float32)
        out[:, pl.ds(k * step, step)] = total.astype(out.dtype)
    for copy in first:
        copy.wait_send()
    for _, copy in second:
        copy.wait_send()


def shards(fs_size, tp_size, tokens, norm_gain, gate_weight, up_weight, down_weight, routes, route_logit):
    experts, depth, width = gate_weight.shape
    _, units, col = down_weight.shape
    rows, features = tokens.shape
    gain_col = norm_gain[None, :, None]
    gate_part = (gate_weight * gain_col).astype(jnp.bfloat16)
    up_part = (up_weight * gain_col).astype(jnp.bfloat16)
    down_part = down_weight.astype(jnp.bfloat16)

    floats = tokens.astype(jnp.float32)
    normed = (floats * lax.rsqrt(jnp.mean(floats * floats, axis=1, keepdims=True) + EPS)).astype(
        jnp.bfloat16
    )
    first_share = jax.nn.sigmoid(route_logit[:, 0] - route_logit[:, 1])
    shares = jnp.stack([first_share, 1.0 - first_share], axis=1)
    named = routes[:, :, None] == jnp.arange(experts, dtype=jnp.int32)[None, None, :]
    weight = jnp.sum(jnp.where(named, shares[:, :, None], 0.0), axis=1)

    half = jnp.bfloat16
    anywhere = pl.BlockSpec(memory_space=pl.ANY)
    dma = pltpu.SemaphoreType.DMA
    gate_shape = jax.ShapeDtypeStruct((experts, features, units), half)
    down_shape = jax.ShapeDtypeStruct((experts, units, features), half)
    far_shape = jax.ShapeDtypeStruct((experts, depth, width), half)
    gate_all, up_all, down_all, _, _ = pl.pallas_call(
        functools.partial(spread, fs_size, tp_size),
        out_shape=(gate_shape, gate_shape, down_shape, far_shape, far_shape),
        in_specs=[anywhere] * 3,
        out_specs=(anywhere,) * 5,
        scratch_shapes=[dma((2, experts))] * 7 + [dma((4,))] * 2,
        compiler_params=pltpu.CompilerParams(has_side_effects=True),
        name="spread",
    )(gate_part, up_part, down_part)

    block = min(units, 512)
    in_wide = pl.BlockSpec((1, features, block), lambda e, j: (e, 0, j))
    in_tall = pl.BlockSpec((1, block, features), lambda e, j: (e, j, 0))
    whole = pl.BlockSpec((rows, features), lambda e, j: (0, 0))
    gate_out, up_out, down_out, part = pl.pallas_call(
        apply_experts,
        grid=(experts, units // block),
        out_shape=(
            gate_shape, gate_shape, down_shape, jax.ShapeDtypeStruct((rows, features), half),
        ),
        in_specs=[
            whole, pl.BlockSpec((rows, experts), lambda e, j: (0, 0)), in_wide, in_wide, in_tall,
        ],
        out_specs=(in_wide, in_wide, in_tall, whole),
        scratch_shapes=[pltpu.VMEM((rows, features), jnp.float32)],
        compiler_params=pltpu.CompilerParams(
            vmem_limit_bytes=VMEM_LIMIT, dimension_semantics=("arbitrary", "arbitrary")
        ),
        name="apply_experts",
    )(normed, weight, gate_all, up_all, down_all)

    highs, mine, chunks = fs_size // 2, rows // fs_size, 4
    step = features // chunks
    vmem = pl.BlockSpec(memory_space=pltpu.VMEM)
    mixed = pl.pallas_call(
        functools.partial(fold, chunks),
        out_shape=jax.ShapeDtypeStruct((mine, features), half),
        in_specs=[vmem],
        out_specs=vmem,
        scratch_shapes=[pltpu.VMEM((chunks, highs, mine, step), half)] * 3
        + [dma((chunks,))] * 2
        + [dma((chunks, highs))] * 2,
        compiler_params=pltpu.CompilerParams(
            has_side_effects=True, vmem_limit_bytes=VMEM_LIMIT // 2
        ),
        name="fold",
    )(part.reshape(highs, 2, mine, features))
    return (gate_out, up_out, down_out, mixed)


def solution(mesh):
    return jax.shard_map(
        functools.partial(shards, mesh.shape["fs"], mesh.shape["tp"]),
        mesh=mesh,
        in_specs=(
            P("tp", None),
            P("fs"),
            P(None, "fs", "tp"),
            P(None, "fs", "tp"),
            P(None, "fs", "tp"),
            P("tp", None),
            P("tp", None),
        ),
        out_specs=(
            P(None, None, "fs"),
            P(None, None, "fs"),
            P(None, "fs", None),
            P(("tp", "fs"), None),
        ),
        check_vma=False,
    )
```

time: 961 us -> 537 us (0.56)
  Pallas kernels: 0 us -> 507 us
  blocking collectives: 347 us -> 0 us
  local copies, waits for them, and re-layouts: 252 us -> 3.58 us
  waiting for transfers between devices: 184 us -> 0 us
  other arithmetic: 118 us -> 26 us
  matrix products: 43.5 us -> 0 us
  between operations: 14 us -> 0.68 us
    pallas_call x0 -> x3, Pallas kernels: none -> 507 us  [the longest x1 369 us: shards(): pl.pallas_call(functools.partial(spread, fs_size, tp_size), out_shape=(ga...]
    all_to_all x4 -> x0, blocking collectives: 347 us -> none  [the longest x1 99.8 us: shards(): lax.all_to_all(up_one, 'fs', split_axis=2, concat_axis=1, tiled=True)]
    reduce_scatter x1 -> x0, waiting for transfers between devices: 118 us -> none  [shards(): lax.psum_scatter(shares[:, 0:1] * first_rows + shares[:, 1:2] * second_ro...]
    all_to_all x4 -> x0, local copies, waits for them, and re-layouts: 112 us -> none  [the longest x1 49.3 us: shards(): lax.all_to_all(up_part, 'tp', split_axis=0, concat_axis=2, tiled=True)]
    unnamed x28 -> x5, local copies, waits for them, and re-layouts: 98.2 us -> 2.63 us
    unnamed x4 -> x0, other arithmetic: 87.2 us -> none
    all_gather x3 -> x0, waiting for transfers between devices: 65.7 us -> none  [the longest x1 65.7 us: shards(): lax.all_gather(gate_mine, 'tp', axis=0, tiled=True)]
    dot_general x2 -> x0, matrix products: 43.5 us -> none  [the longest x1 27.2 us: shards(): jnp.einsum('ecf,efd->ecd', hidden, down_out, preferred_element_type=jnp.f...]
  transfers between devices with their start and end apart: 4 -> 0, of which waited for: 2 -> 0; matrix products, arithmetic and copies ran while one was open for 17% -> 0% of each run, Pallas kernels for 0% -> 0%
where the time goes in v1:
time: 537 us
  Pallas kernels  507 us (94%)
  other arithmetic  26 us (5%)
    pallas_call x1, Pallas kernels, shards(): pl.pallas_call(functools.partial(spread, fs_size, tp_size), out_shape=(ga...  369 us
    pallas_call x1, Pallas kernels, shards(): pl.pallas_call(functools.partial(fold, chunks), out_shape=jax.ShapeDtypeS...  82.9 us
    pallas_call x1, Pallas kernels, shards(): pl.pallas_call(apply_experts, grid=(experts, units // block), out_shape=(...  54.9 us
    convert_element_type x1, other arithmetic, shards(): up_part = (up_weight * gain_col).astype(jnp.bfloat16)  11.8 us

profile of v1, /device:TPU:0, one launch (start us, length us, event | category | flops | bytes accessed | tf_op | source)
XLA Modules:
  0.0 536.9 jit_solution(13598115814696104244)
XLA Ops:
  0.6 2.6 fusion
  3.2 0.8 broadcast_subtract_fusion
  4.0 0.7 select_reduce_fusion
  4.7 0.9 copy.13.weight
  5.7 4.1 fusion.1.x
  9.8 0.0 copy-start.1
  9.8 5.9 %convert_element_type.19.down = bf16[4,1024,512]{2,1,0:T(8,128)(2,1)} convert(f32[4,1024,512]{2,1,0:T(8,128)} %param.11) | non-fusion elementwise | flops 2097152 | bytes 12582912 | tf_op jit(solution)/shard_map/convert_element_type | solution.py:217
  15.7 0.0 copy-done.1
  15.7 11.8 %multiply_convert_fusion = (bf16[4,256,2048]{2,1,0:T(8,128)(2,1)}, bf16[4,256,2048]{2,1,0:T(8,128)(2,1)}) fusion(f32[4,256,2048]{2,1,0:T(8,128)} %param.10, f32[256]{0:T(256)S(1)} %copy-done.1, f32[4,256,2048]{2,1,0:T(8,128)} %param.9), kind=kLoop, calls=%fused_computation | loop fusion | flops 8388608 | bytes 25166848 | tf_op jit(solution)/shard_map/convert_element_type | solution.py:216
  27.6 368.8 %spread.1 = (bf16[4,2048,1024]{2,1,0:T(8,128)(2,1)}, bf16[4,2048,1024]{2,1,0:T(8,128)(2,1)}, bf16[4,1024,2048]{2,1,0:T(8,128)(2,1)}, bf16[4,256,2048]{2,1,0:T(8,128)(2,1)}, bf16[4,256,2048]{2,1,0:T(8,128)(2,1)}) custom-call(bf16[4,256,2048]{2,1,0:T(8,128)(2,1)} %get-tuple-element.21.gate, bf16[4,256,2048]{2,1,0:T(8,128)(2,1)} %get-tuple-element.20.up, ...), custom_call_target="tpu_custom_call" | custom-call | tf_op jit(solution)/shard_map/spread/pallas_call | solution.py:234
  396.4 54.9 %apply_experts.1 = (bf16[4,2048,1024]{2,1,0:T(8,128)(2,1)}, bf16[4,2048,1024]{2,1,0:T(8,128)(2,1)}, bf16[4,1024,2048]{2,1,0:T(8,128)(2,1)}, bf16[768,2048]{1,0:T(8,128)(2,1)}) custom-call(bf16[768,2048]{1,0:T(8,128)(2,1)} %fusion.1.x, f32[768,4]{1,0:T(8,128)} %copy.13.weight, bf16[4,2048,1024]{2,1,0:T(8,128)(2,1)} %get-tuple-element.11.gate, ...), custom_call_target="tpu_custom_call" | custom-call | tf_op jit(solution)/shard_map/apply_experts/pallas_call | solution.py:248
  451.3 0.0 copy-start
  451.3 1.9 copy-done
  453.2 82.9 %fold.1 = bf16[96,2048]{1,0:T(8,128)(2,1)S(1)} custom-call(bf16[4,2,96,2048]{3,2,1,0:T(8,128)(2,1)S(1)} %bitcast.1), custom_call_target="tpu_custom_call" | custom-call | tf_op jit(solution)/shard_map/fold/pallas_call | solution.py:268
  536.1 0.7 copy.15
  (2 shorter events, 0.0 us)
Async XLA Ops:
  9.8 5.9 %copy-start.1 = (f32[256]{0:T(256)S(1)}, f32[256]{0:T(256)}, u32[]{:S(2)}) copy-start(f32[256]{0:T(256)} %param.8) | copy-start | bytes 3076
  451.3 1.9 copy-start
